TPU v7x, 512 devices: a whole 4x4x16 slice. The times are simulated.
512 devices in a mesh: fs: 16 (over y, x), tp: 32 (over z, core).
Axes of the slice: x: 4, y: 4, z: 16, core: 2. Of those that a mesh axis runs over, the one named last changes fastest.
Arguments:
- value_input: bfloat16 [32768, 2048], P('fs', 'tp'), may hold values from -50 to 50
- value_cotangent: bfloat16 [32768, 512], P('fs'), may hold values from -6 to 6
- value_factor: bfloat16 [512, 128], replicated, may hold values from -10 to 10
- value_master: float32 [512, 2048], P('fs', 'tp'), may hold values from -0.125 to 0.125
- value_first: float32 [128, 2048], P('fs', 'tp'), may hold values from -4 to 4
- value_second: float32 [128, 2048], P('fs', 'tp'), may hold values from 0.01 to 0.2
- mixed_heads: bfloat16 [32768, 1024], P('fs', 'tp'), may hold values from -6 to 6
- output_cotangent: bfloat16 [32768, 2048], P('fs', 'tp'), may hold values from -50 to 50
- output_factor: bfloat16 [1024, 128], replicated, may hold values from -10 to 10
- output_master: float32 [1024, 2048], P('fs', 'tp'), may hold values from -0.1875 to 0.1875
- output_first: float32 [128, 2048], P('fs', 'tp'), may hold values from -4 to 4
- output_second: float32 [128, 2048], P('fs', 'tp'), may hold values from 0.01 to 0.2
Outputs:
- value_step: float32 [512, 2048], P('fs', 'tp')
- value_new_master: float32 [512, 2048], P('fs', 'tp')
- value_copy: bfloat16 [512, 2048], P(None, 'tp')
- value_first_new: float32 [128, 2048], P('fs', 'tp')
- value_second_new: float32 [128, 2048], P('fs', 'tp')
- output_step: float32 [1024, 2048], P('fs', 'tp')
- output_new_master: float32 [1024, 2048], P('fs', 'tp')
- output_copy: bfloat16 [1024, 2048], P(None, 'tp')
- output_first_new: float32 [128, 2048], P('fs', 'tp')
- output_second_new: float32 [128, 2048], P('fs', 'tp')
All inputs are finite; a program needn't handle non-finite values.
Results may differ from a plain program's by a relative error of at most 0.001.
Values may be sent and summed in bfloat16 or wider, within the bound.
A program may use at most 64 MiB of HBM per device.

v0:
```python
import jax
import jax.numpy as jnp
from jax import lax
from jax.sharding import Mesh
from jax.sharding import PartitionSpec as P

FS = ("fs_0", "fs_1")
TP = ("tp_0", "tp_1")
FS_TP = ("fs_0", "fs_1", "tp_0", "tp_1")
highest = lax.Precision.HIGHEST


def split_up(x, dim, count):
    dims = x.shape
    tiles = x.reshape(*dims[:dim], count, dims[dim] // count, *dims[dim + 1 :])
    return jnp.moveaxis(tiles, dim, 0)


def summed_on_arrival(x, axis, dim):
    count = lax.axis_size(axis)
    tiles = lax.all_to_all(split_up(x, dim, count), axis, 0, 0, tiled=True)
    return jnp.sum(tiles, axis=0)


def by_axis(x, axes):
    for axis in axes:
        x = lax.psum(x, axis)
    return x


def in_one_piece(arrays, axis, dim, along):
    both = jnp.concatenate(arrays, axis=along)
    whole, at, outs = (lax.all_gather(both, axis, axis=dim, tiled=True), 0, [])
    for a in arrays:
        outs.append(lax.slice_in_dim(whole, at, at + a.shape[along], axis=along))
        at += a.shape[along]
    return tuple(outs)


def joined_along(tiles, dim):
    dims = list(tiles.shape[1:])
    dims[dim] *= tiles.shape[0]
    return jnp.moveaxis(tiles, 0, dim).reshape(dims)


def gather_packed(arrays, axis, dims):
    flat = jnp.concatenate([a.reshape(-1) for a in arrays])
    lines, at, outs = (lax.all_gather(flat, axis), 0, [])
    for a, dim in zip(arrays, dims):
        tiles = lines[:, at : at + a.size].reshape(-1, *a.shape)
        outs.append(joined_along(tiles, dim))
        at += a.size
    return tuple(outs)


def tokens_exact(left, right):
    return lax.dot_general(
        left, right, (((0,), (0,)), ((), ())), precision=highest, preferred_element_type=jnp.float32
    )


def moment_update(projected, scale, first, second):
    scaled = scale * projected
    first_new = 0.9 * first + 0.1 * scaled
    second_new = 0.95 * second + 0.05 * scaled * scaled
    direction = first_new / (jnp.sqrt(second_new) + 1e-08)
    return (first_new, second_new, direction)


def project_both(value_image, output_image, value_input, output_cotangent, band):
    value_wide = value_input.astype(jnp.float32)
    output_wide = output_cotangent.astype(jnp.float32)
    columns = value_input.shape[1]
    blocks = 2 * band * lax.axis_size(FS) // (2 * band)
    value_term = tokens_exact(value_image, value_wide).reshape(blocks, band, columns)
    output_term = tokens_exact(output_image, output_wide).reshape(blocks, band, columns)
    paired = summed_on_arrival(
        jnp.stack([value_term, output_term], axis=1).reshape(2 * band * lax.axis_size(FS), columns),
        FS,
        0,
    )
    return (paired[:band], paired[band:])


def on_device(
    value_input,
    value_cotangent,
    value_factor,
    value_master,
    value_first,
    value_second,
    mixed_heads,
    output_cotangent,
    output_factor,
    output_master,
    output_first,
    output_second,
):
    fs_count = lax.axis_size(FS)
    fs_place = lax.axis_index(FS)
    rank = value_factor.shape[1]
    band = rank // fs_count
    columns = value_input.shape[1]
    value_rows = value_master.shape[0]
    output_rows = output_master.shape[0]
    value_block = lax.dynamic_slice_in_dim(
        value_factor, fs_place * value_rows, value_rows, 0
    ).astype(jnp.float32)
    output_block = lax.dynamic_slice_in_dim(
        output_factor, fs_place * output_rows, output_rows, 0
    ).astype(jnp.float32)
    value_image = jnp.dot(value_cotangent, value_factor, preferred_element_type=jnp.float32)
    heads_whole = lax.all_gather(mixed_heads, TP, axis=1, tiled=True)
    output_image = jnp.dot(heads_whole, output_factor, preferred_element_type=jnp.float32)
    value_proj, output_proj = project_both(
        value_image, output_image, value_input, output_cotangent, band
    )
    total_count = rank * columns * lax.axis_size(TP)
    value_square, output_square = (
        by_axis(jnp.sum(value_proj * value_proj), FS_TP),
        by_axis(jnp.sum(output_proj * output_proj), FS_TP),
    )
    value_scale = lax.rsqrt(value_square / total_count + 1e-06)
    output_scale = lax.rsqrt(output_square / total_count + 1e-06)
    value_first_new, value_second_new, value_dir = moment_update(
        value_proj, value_scale, value_first, value_second
    )
    output_first_new, output_second_new, output_dir = moment_update(
        output_proj, output_scale, output_first, output_second
    )
    value_dir_all, output_dir_all = in_one_piece((value_dir, output_dir), FS, 0, 1)
    value_step = jnp.dot(
        value_block, value_dir_all, precision=highest, preferred_element_type=jnp.float32
    )
    output_step = jnp.dot(
        output_block, output_dir_all, precision=highest, preferred_element_type=jnp.float32
    )
    value_new = value_master - 0.002 * value_step
    output_new = output_master - 0.002 * output_step
    value_copy, output_copy = gather_packed(
        (value_new.astype(jnp.bfloat16), output_new.astype(jnp.bfloat16)), FS, (0, 0)
    )
    return (
        value_step,
        value_new,
        value_copy,
        value_first_new,
        value_second_new,
        output_step,
        output_new,
        output_copy,
        output_first_new,
        output_second_new,
    )


def solution(mesh):
    split = Mesh(mesh.devices.reshape(4, 4, 16, 2), ("fs_0", "fs_1", "tp_0", "tp_1"))
    return jax.shard_map(
        on_device,
        mesh=split,
        in_specs=(
            P(FS, TP),
            P(FS, None),
            P(),
            P(FS, TP),
            P(FS, TP),
            P(FS, TP),
            P(FS, TP),
            P(FS, TP),
            P(),
            P(FS, TP),
            P(FS, TP),
            P(FS, TP),
        ),
        out_specs=(
            P(FS, TP),
            P(FS, TP),
            P(None, TP),
            P(FS, TP),
            P(FS, TP),
            P(FS, TP),
            P(FS, TP),
            P(None, TP),
            P(FS, TP),
            P(FS, TP),
        ),
        check_vma=False,
    )
```

profile of v0, /device:TPU:4, one launch (start us, length us, event | category | flops | bytes accessed | tf_op | source)
XLA Modules:
  0.0 218.8 jit_solution(8862395068048219859)
XLA Ops:
  7.2 0.0 all-gather.3.cloned.1.call-start
  7.2 0.7 all-gather.3.cloned.1.call-update
  7.9 0.8 copy-done
  8.8 1.6 fusion.14
  10.4 2.0 convolution_bitcast_fusion.1
  12.5 75.5 %all-gather.3.cloned.1.call-done = bf16[2048,1024]{0,1:T(8,128)(2,1)} async-done(((bf16[2048,32]{0,1:T(8,128)(2,1)}), bf16[2048,1024]{0,1:T(8,128)(2,1)}) %all-gather.3.cloned.1.call-update) | async-done | bytes 4194320 | tf_op jit(solution)/shard_map/all_gather | solution.py:113
  88.0 3.5 %fusion.15 = f32[2048,128]{1,0:T(8,128)S(1)} fusion(bf16[2048,1024]{0,1:T(8,128)(2,1)} %all-gather.3.cloned.1.call-done, bf16[1024,128]{1,0:T(8,128)(2,1)S(1)} %copy-done.1), kind=kOutput, calls=%fused_computation.31 | convolution fusion | flops 536870912 | bytes 5505024 | tf_op jit(solution)/shard_map/dot_general | solution.py:114
  91.5 1.0 convolution_bitcast_fusion
  92.5 0.8 reshape.29
  93.2 7.3 %all-to-all-start = ((f32[16,1,1024]{2,1,0:T(1,128)}), f32[16,1,1024]{2,1,0:T(1,128)S(1)}, u32[]{:S(2)}, u32[]{:S(2)}) async-start(f32[16,1,1024]{2,1,0:T(1,128)} %reshape.29), calls=%async_computation | async-start | bytes 131072 | tf_op jit(solution)/shard_map/all_to_all | solution.py:21
  100.5 5.5 %all-to-all-done = f32[16,1,1024]{2,1,0:T(1,128)S(1)} async-done(((f32[16,1,1024]{2,1,0:T(1,128)}), f32[16,1,1024]{2,1,0:T(1,128)S(1)}, u32[]{:S(2)}, u32[]{:S(2)}) %all-to-all-start) | async-done | bytes 65568 | tf_op jit(solution)/shard_map/all_to_all | solution.py:21
  106.0 0.5 broadcast.38
  106.6 0.8 reduce
  107.4 0.1 reshape.30
  107.5 0.6 multiply_reduce_fusion.1
  108.1 9.5 %all-reduce.2 = (f32[]{:T(128)}, f32[]{:T(128)}) all-reduce(f32[]{:T(128)} %get-tuple-element.31, f32[]{:T(128)} %get-tuple-element.30), channel_id=1, replica_groups=mesh['fs_0'=4,'fs_1'=4,'tp_0'=16,'tp_1'=2] {'fs_0'}, use_global_device_ids=true, to_apply=%region_7.0 | all-reduce | flops 2 | bytes 16 | tf_op jit(solution)/shard_map/psum | solution.py:27
  117.6 9.1 %all-reduce.1 = (f32[]{:T(128)}, f32[]{:T(128)}) all-reduce(f32[]{:T(128)} %get-tuple-element.36, f32[]{:T(128)} %get-tuple-element.37), channel_id=1, replica_groups=mesh['fs_0'=4,'fs_1'=4,'tp_0'=16,'tp_1'=2] {'fs_1'}, use_global_device_ids=true, to_apply=%region_8.0 | all-reduce | flops 2 | bytes 16 | tf_op jit(solution)/shard_map/psum | solution.py:27
  126.6 30.3 %all-reduce = (f32[]{:T(128)}, f32[]{:T(128)}) all-reduce(f32[]{:T(128)} %get-tuple-element.34, f32[]{:T(128)} %get-tuple-element.35), channel_id=1, replica_groups=mesh['fs_0'=4,'fs_1'=4,'tp_0'=16,'tp_1'=2] {'tp_0'}, use_global_device_ids=true, to_apply=%region_9.0 | all-reduce | flops 2 | bytes 16 | tf_op jit(solution)/shard_map/psum | solution.py:27
  156.9 3.1 %all-reduce.3 = (f32[]{:T(128)}, f32[]{:T(128)}) all-reduce(f32[]{:T(128)} %get-tuple-element.32, f32[]{:T(128)} %get-tuple-element.33), channel_id=1, replica_groups=mesh['fs_0'=4,'fs_1'=4,'tp_0'=16,'tp_1'=2] {'tp_1'}, use_global_device_ids=true, to_apply=%region_10.0 | all-reduce | flops 2 | bytes 16 | tf_op jit(solution)/shard_map/psum | solution.py:27
  161.4 0.6 add_divide_fusion.1
  162.0 0.1 pad_maximum_fusion.2
  162.1 22.1 %all_gather.13 = f32[128,128]{1,0:T(8,128)S(1)} all-gather(f32[8,128]{1,0:T(8,128)S(1)} %pad_maximum_fusion.2), channel_id=1, replica_groups=mesh['fs_0'=4,'fs_1'=4,'tp_0'=16,'tp_1'=2] {'fs_0','fs_1'}, dimensions={0}, use_global_device_ids=true | all-gather | bytes 69632 | tf_op jit(solution)/shard_map/all_gather | solution.py:33
  184.2 0.9 fusion.11
  185.1 0.1 reshape.27
  185.2 1.5 fusion.10
  186.6 0.1 reshape.26
  186.7 23.2 %all-gather = bf16[98304]{0:T(1024)(128)(2,1)S(1)} all-gather(bf16[6144]{0:T(1024)(128)(2,1)S(1)} %pad_maximum_fusion.1), channel_id=2, replica_groups=mesh['fs_0'=4,'fs_1'=4,'tp_0'=16,'tp_1'=2] {'fs_0','fs_1'}, dimensions={0}, use_global_device_ids=true | all-gather | bytes 208896 | tf_op jit(solution)/shard_map/all_gather | solution.py:48
  209.9 0.1 reshape.28
  210.0 0.2 reshape_reshape.11
  210.3 0.8 copy.31
  211.0 0.2 reshape_reshape.10
  211.2 0.7 copy.30
  (22 shorter events, 0.1 us)
Async XLA Ops:
  7.2 1.6 copy-start
  7.2 80.8 %copy-start.1 = (bf16[1024,128]{1,0:T(8,128)(2,1)S(1)}, bf16[1024,128]{1,0:T(8,128)(2,1)}, u32[]{:S(2)}) copy-start(bf16[1024,128]{1,0:T(8,128)(2,1)} %param.20) | copy-start | bytes 786436
  7.2 80.8 %all-gather.3.cloned.1.call-start = ((), (), s32[]{:S(2)}) async-start(), calls=%async_computation.1 | async-start | bytes 4325376 | tf_op jit(solution)/shard_map/all_gather | solution.py:113
  10.4 81.1 %copy-start.2 = (bf16[2048,64]{0,1:T(8,128)(2,1)S(1)}, bf16[2048,64]{0,1:T(8,128)(2,1)}, u32[]{:S(2)}) copy-start(bf16[2048,64]{0,1:T(8,128)(2,1)} %param.19) | copy-start | bytes 786436
  12.4 149.0 %copy-start.5 = (f32[8,64]{1,0:T(8,128)S(1)}, f32[8,64]{1,0:T(8,128)}, u32[]{:S(2)}) copy-start(f32[8,64]{1,0:T(8,128)} %param.17) | copy-start | bytes 6148
  12.4 149.0 %copy-start.6 = (f32[8,64]{1,0:T(8,128)S(1)}, f32[8,64]{1,0:T(8,128)}, u32[]{:S(2)}) copy-start(f32[8,64]{1,0:T(8,128)} %param.16) | copy-start | bytes 6148
  12.4 149.0 %copy-start.7 = (f32[8,64]{1,0:T(8,128)S(1)}, f32[8,64]{1,0:T(8,128)}, u32[]{:S(2)}) copy-start(f32[8,64]{1,0:T(8,128)} %param.23) | copy-start | bytes 6148
  12.4 149.0 %copy-start.8 = (f32[8,64]{1,0:T(8,128)S(1)}, f32[8,64]{1,0:T(8,128)}, u32[]{:S(2)}) copy-start(f32[8,64]{1,0:T(8,128)} %param.22) | copy-start | bytes 6148
  12.4 171.8 %copy-start.3 = (f32[64,64]{1,0:T(8,128)S(1)}, f32[64,64]{1,0:T(8,128)}, u32[]{:S(2)}) copy-start(f32[64,64]{1,0:T(8,128)} %param.21) | copy-start | bytes 49156
  12.4 172.7 %copy-start.4 = (f32[32,64]{1,0:T(8,128)S(1)}, f32[32,64]{1,0:T(8,128)}, u32[]{:S(2)}) copy-start(f32[32,64]{1,0:T(8,128)} %param.15) | copy-start | bytes 24580
  93.2 12.8 %all-to-all-start = ((f32[16,1,1024]{2,1,0:T(1,128)}), f32[16,1,1024]{2,1,0:T(1,128)S(1)}, u32[]{:S(2)}, u32[]{:S(2)}) async-start(f32[16,1,1024]{2,1,0:T(1,128)} %reshape.29), calls=%async_computation | async-start | bytes 131072 | tf_op jit(solution)/shard_map/all_to_all | solution.py:21
Sparse Core Ops, SparseCore 0:
  10.1 77.7 all-gather.2
where the time goes:
time: 219 us
  blocking collectives  97.2 us (44%)
  waiting for transfers between devices  81.7 us (37%)
  between operations  15.6 us (7%)
  matrix products  10.4 us (5%)
  starting transfers between devices  7.3 us (3%)
  local copies, waits for them, and re-layouts  4.46 us (2%)
    all_gather x1, waiting for transfers between devices, on_device(): heads_whole = lax.all_gather(mixed_heads, TP, axis=1, tiled=True)  75.5 us
    psum x4, blocking collectives, by_axis(): x = lax.psum(x, axis)  51.9 us
    all_gather x1, blocking collectives, gather_packed(): lines, at, outs = (lax.all_gather(flat, axis), 0, [])  23.2 us
    all_gather x1, blocking collectives, in_one_piece(): whole, at, outs = (lax.all_gather(both, axis, axis=dim, tiled=True), 0, [])  22.1 us
    all_to_all x1, starting transfers between devices, summed_on_arrival(): tiles = lax.all_to_all(split_up(x, dim, count), axis, 0, 0, tiled=True)  7.27 us
    all_to_all x1, waiting for transfers between devices, summed_on_arrival(): tiles = lax.all_to_all(split_up(x, dim, count), axis, 0, 0, tiled=True)  5.54 us
  transfers between devices with their start and end apart: 2, of which 2 were waited for; matrix products, arithmetic and copies ran while one was open for 2% of the time, Pallas kernels for 0%

commit v1 on v0

--- a/solution.py
+++ b/solution.py
@@ -110,7 +110,9 @@
         output_factor, fs_place * output_rows, output_rows, 0
     ).astype(jnp.float32)
     value_image = jnp.dot(value_cotangent, value_factor, preferred_element_type=jnp.float32)
-    heads_whole = lax.all_gather(mixed_heads, TP, axis=1, tiled=True)
+    heads_whole = jnp.concatenate(
+        lax.all_to_all(jnp.stack([mixed_heads] * lax.axis_size(TP)), TP, 0, 0), axis=1
+    )
     output_image = jnp.dot(heads_whole, output_factor, preferred_element_type=jnp.float32)
     value_proj, output_proj = project_both(
         value_image, output_image, value_input, output_cotangent, band

time: 219 us -> 333 us (1.52)
  waiting for transfers between devices: 81.7 us -> 187 us
  starting transfers between devices: 7.3 us -> 23.2 us
  between operations: 15.6 us -> 2.23 us
  blocking collectives: 97.2 us -> 103 us
    all_to_all x0 -> x1, waiting for transfers between devices: none -> 182 us  [on_device(): lax.all_to_all(jnp.stack([mixed_heads] * lax.axis_size(TP)), TP, 0, 0)]
    all_gather x1 -> x0, waiting for transfers between devices: 75.5 us -> none  [on_device(): heads_whole = lax.all_gather(mixed_heads, TP, axis=1, tiled=True)]
    all_to_all x0 -> x1, starting transfers between devices: none -> 15.7 us  [on_device(): lax.all_to_all(jnp.stack([mixed_heads] * lax.axis_size(TP)), TP, 0, 0)]
    psum x4, blocking collectives: 51.9 us -> 57.3 us  [by_axis(): x = lax.psum(x, axis)]
    another operation x0 -> x1, local copies, waits for them, and re-layouts: none -> 3.54 us  [on_device(): jnp.stack([mixed_heads] * lax.axis_size(TP))]
  transfers between devices with their start and end apart: 2 -> 2, of which waited for: 2 -> 2; matrix products, arithmetic and copies ran while one was open for 2% -> 1% of each run, Pallas kernels for 0% -> 0%
where the time goes in v1:
time: 333 us; the launch traced here: 332 us
  waiting for transfers between devices  187 us (56%)
  blocking collectives  103 us (31%)
  starting transfers between devices  23.2 us (7%)
  matrix products  7.85 us (2%)
  local copies, waits for them, and re-layouts  7.17 us (2%)
    all_to_all x1, waiting for transfers between devices, on_device(): lax.all_to_all(jnp.stack([mixed_heads] * lax.axis_size(TP)), TP, 0, 0)  182 us
    psum x4, blocking collectives, by_axis(): x = lax.psum(x, axis)  57.3 us
    all_gather x1, blocking collectives, gather_packed(): lines, at, outs = (lax.all_gather(flat, axis), 0, [])  23.2 us
    all_gather x1, blocking collectives, in_one_piece(): whole, at, outs = (lax.all_gather(both, axis, axis=dim, tiled=True), 0, [])  22.1 us
    all_to_all x1, starting transfers between devices, on_device(): lax.all_to_all(jnp.stack([mixed_heads] * lax.axis_size(TP)), TP, 0, 0)  15.7 us
    all_to_all x1, starting transfers between devices, summed_on_arrival(): tiles = lax.all_to_all(split_up(x, dim, count), axis, 0, 0, tiled=True)  7.45 us
  transfers between devices with their start and end apart: 2, of which 2 were waited for; matrix products, arithmetic and copies ran while one was open for 1% of the time, Pallas kernels for 0%

profile of v1, /device:TPU:4, one launch (start us, length us, event | category | flops | bytes accessed | tf_op | source)
XLA Modules:
  0.0 332.4 jit_solution(14355748823505048202)
XLA Ops:
  0.6 0.0 copy-start
  0.7 3.5 %stack.4 = bf16[32,2048,32]{1,2,0:T(8,128)(2,1)} broadcast(bf16[2048,32]{0,1:T(8,128)(2,1)} %param.18), dimensions={1,2} | broadcast | bytes 4325376 | tf_op jit(solution)/shard_map/stack | solution.py:114
  4.2 15.7 %all-to-all-start = ((bf16[32,2048,32]{1,2,0:T(8,128)(2,1)}), bf16[32,2048,32]{1,2,0:T(8,128)(2,1)}, u32[]{:S(2)}, u32[]{:S(2)}) async-start(bf16[32,2048,32]{1,2,0:T(8,128)(2,1)} %stack.4), calls=%async_computation | async-start | bytes 8388608 | tf_op jit(solution)/shard_map/all_to_all | solution.py:114
  20.0 0.7 fusion.14
  20.7 1.0 convolution_bitcast_fusion.1
  21.7 181.7 %all-to-all-done = bf16[32,2048,32]{1,2,0:T(8,128)(2,1)} async-done(((bf16[32,2048,32]{1,2,0:T(8,128)(2,1)}), bf16[32,2048,32]{1,2,0:T(8,128)(2,1)}, u32[]{:S(2)}, u32[]{:S(2)}) %all-to-all-start) | async-done | bytes 4194336 | tf_op jit(solution)/shard_map/all_to_all | solution.py:114
  203.5 3.5 %fusion.15 = f32[2048,128]{1,0:T(8,128)S(1)} fusion(bf16[2048,1024]{0,1:T(8,128)(2,1)} %bitcast.2, bf16[1024,128]{1,0:T(8,128)(2,1)S(1)} %copy-done.1), kind=kOutput, calls=%fused_computation.31 | convolution fusion | flops 536870912 | bytes 5505024 | tf_op jit(solution)/shard_map/dot_general | solution.py:116
  207.0 1.0 convolution_bitcast_fusion
  208.1 0.8 reshape.39
  208.8 7.4 %all-to-all-start.1 = ((f32[16,1,1024]{2,1,0:T(1,128)}), f32[16,1,1024]{2,1,0:T(1,128)S(1)}, u32[]{:S(2)}, u32[]{:S(2)}) async-start(f32[16,1,1024]{2,1,0:T(1,128)} %reshape.39), calls=%async_computation.1 | async-start | bytes 131072 | tf_op jit(solution)/shard_map/all_to_all | solution.py:21
  216.3 5.5 %all-to-all-done.1 = f32[16,1,1024]{2,1,0:T(1,128)S(1)} async-done(((f32[16,1,1024]{2,1,0:T(1,128)}), f32[16,1,1024]{2,1,0:T(1,128)S(1)}, u32[]{:S(2)}, u32[]{:S(2)}) %all-to-all-start.1) | async-done | bytes 65568 | tf_op jit(solution)/shard_map/all_to_all | solution.py:21
  221.8 0.5 broadcast.40
  222.3 0.8 reduce
  223.1 0.1 reshape.40
  223.2 0.6 multiply_reduce_fusion.1
  223.9 9.5 %all-reduce.2 = (f32[]{:T(128)}, f32[]{:T(128)}) all-reduce(f32[]{:T(128)} %get-tuple-element.31, f32[]{:T(128)} %get-tuple-element.30), channel_id=1, replica_groups=mesh['fs_0'=4,'fs_1'=4,'tp_0'=16,'tp_1'=2] {'fs_0'}, use_global_device_ids=true, to_apply=%region_7.0 | all-reduce | flops 2 | bytes 16 | tf_op jit(solution)/shard_map/psum | solution.py:27
  233.4 9.1 %all-reduce.1 = (f32[]{:T(128)}, f32[]{:T(128)}) all-reduce(f32[]{:T(128)} %get-tuple-element.36, f32[]{:T(128)} %get-tuple-element.37), channel_id=1, replica_groups=mesh['fs_0'=4,'fs_1'=4,'tp_0'=16,'tp_1'=2] {'fs_1'}, use_global_device_ids=true, to_apply=%region_8.0 | all-reduce | flops 2 | bytes 16 | tf_op jit(solution)/shard_map/psum | solution.py:27
  242.4 35.6 %all-reduce = (f32[]{:T(128)}, f32[]{:T(128)}) all-reduce(f32[]{:T(128)} %get-tuple-element.34, f32[]{:T(128)} %get-tuple-element.35), channel_id=1, replica_groups=mesh['fs_0'=4,'fs_1'=4,'tp_0'=16,'tp_1'=2] {'tp_0'}, use_global_device_ids=true, to_apply=%region_9.0 | all-reduce | flops 2 | bytes 16 | tf_op jit(solution)/shard_map/psum | solution.py:27
  278.0 3.1 all-reduce.3
  282.5 0.6 add_divide_fusion.1
  283.1 0.1 pad_maximum_fusion.2
  283.2 22.1 %all_gather.9 = f32[128,128]{1,0:T(8,128)S(1)} all-gather(f32[8,128]{1,0:T(8,128)S(1)} %pad_maximum_fusion.2), channel_id=1, replica_groups=mesh['fs_0'=4,'fs_1'=4,'tp_0'=16,'tp_1'=2] {'fs_0','fs_1'}, dimensions={0}, use_global_device_ids=true | all-gather | bytes 69632 | tf_op jit(solution)/shard_map/all_gather | solution.py:33
  305.3 0.9 fusion.11
  306.2 0.1 reshape.37
  306.3 0.8 fusion.10
  307.1 0.1 reshape.36
  307.2 23.2 %all-gather = bf16[98304]{0:T(1024)(128)(2,1)S(1)} all-gather(bf16[6144]{0:T(1024)(128)(2,1)S(1)} %pad_maximum_fusion.1), channel_id=2, replica_groups=mesh['fs_0'=4,'fs_1'=4,'tp_0'=16,'tp_1'=2] {'fs_0','fs_1'}, dimensions={0}, use_global_device_ids=true | all-gather | bytes 208896 | tf_op jit(solution)/shard_map/all_gather | solution.py:48
  330.3 0.1 reshape.38
  330.4 0.2 reshape_reshape.11
  330.7 0.8 copy.32
  331.5 0.2 reshape_reshape.10
  331.6 0.7 copy.31
  (26 shorter events, 0.1 us)
Async XLA Ops:
  0.6 19.3 %copy-start = (bf16[2048,512]{1,0:T(8,128)(2,1)S(1)}, bf16[2048,512]{1,0:T(8,128)(2,1)}, u32[]{:S(2)}) copy-start(bf16[2048,512]{1,0:T(8,128)(2,1)} %param.13) | copy-start | bytes 6291460
  4.2 15.8 %copy-start.4 = (bf16[512,128]{1,0:T(8,128)(2,1)S(1)}, bf16[512,128]{1,0:T(8,128)(2,1)}, u32[]{:S(2)}) copy-start(bf16[512,128]{1,0:T(8,128)(2,1)} %param.14) | copy-start | bytes 393220
  4.2 16.5 %copy-start.2 = (bf16[2048,64]{0,1:T(8,128)(2,1)S(1)}, bf16[2048,64]{0,1:T(8,128)(2,1)}, u32[]{:S(2)}) copy-start(bf16[2048,64]{0,1:T(8,128)(2,1)} %param.12) | copy-start | bytes 786436
  4.2 199.2 %all-to-all-start = ((bf16[32,2048,32]{1,2,0:T(8,128)(2,1)}), bf16[32,2048,32]{1,2,0:T(8,128)(2,1)}, u32[]{:S(2)}, u32[]{:S(2)}) async-start(bf16[32,2048,32]{1,2,0:T(8,128)(2,1)} %stack.4), calls=%async_computation | async-start | bytes 8388608 | tf_op jit(solution)/shard_map/all_to_all | solution.py:114
  20.0 183.5 %copy-start.1 = (bf16[1024,128]{1,0:T(8,128)(2,1)S(1)}, bf16[1024,128]{1,0:T(8,128)(2,1)}, u32[]{:S(2)}) copy-start(bf16[1024,128]{1,0:T(8,128)(2,1)} %param.20) | copy-start | bytes 786436
  20.7 186.3 %copy-start.3 = (bf16[2048,64]{0,1:T(8,128)(2,1)S(1)}, bf16[2048,64]{0,1:T(8,128)(2,1)}, u32[]{:S(2)}) copy-start(bf16[2048,64]{0,1:T(8,128)(2,1)} %param.19) | copy-start | bytes 786436
  203.5 79.0 %copy-start.7 = (f32[8,64]{1,0:T(8,128)S(1)}, f32[8,64]{1,0:T(8,128)}, u32[]{:S(2)}) copy-start(f32[8,64]{1,0:T(8,128)} %param.17) | copy-start | bytes 6148
  203.5 79.0 %copy-start.8 = (f32[8,64]{1,0:T(8,128)S(1)}, f32[8,64]{1,0:T(8,128)}, u32[]{:S(2)}) copy-start(f32[8,64]{1,0:T(8,128)} %param.16) | copy-start | bytes 6148
  203.5 79.1 %copy-start.9 = (f32[8,64]{1,0:T(8,128)S(1)}, f32[8,64]{1,0:T(8,128)}, u32[]{:S(2)}) copy-start(f32[8,64]{1,0:T(8,128)} %param.23) | copy-start | bytes 6148
  203.5 79.1 %copy-start.10 = (f32[8,64]{1,0:T(8,128)S(1)}, f32[8,64]{1,0:T(8,128)}, u32[]{:S(2)}) copy-start(f32[8,64]{1,0:T(8,128)} %param.22) | copy-start | bytes 6148
  203.5 101.9 %copy-start.5 = (f32[64,64]{1,0:T(8,128)S(1)}, f32[64,64]{1,0:T(8,128)}, u32[]{:S(2)}) copy-start(f32[64,64]{1,0:T(8,128)} %param.21) | copy-start | bytes 49156
  203.5 102.8 %copy-start.6 = (f32[32,64]{1,0:T(8,128)S(1)}, f32[32,64]{1,0:T(8,128)}, u32[]{:S(2)}) copy-start(f32[32,64]{1,0:T(8,128)} %param.15) | copy-start | bytes 24580
  208.8 13.0 %all-to-all-start.1 = ((f32[16,1,1024]{2,1,0:T(1,128)}), f32[16,1,1024]{2,1,0:T(1,128)S(1)}, u32[]{:S(2)}, u32[]{:S(2)}) async-start(f32[16,1,1024]{2,1,0:T(1,128)} %reshape.39), calls=%async_computation.1 | async-start | bytes 131072 | tf_op jit(solution)/shard_map/all_to_all | solution.py:21
